TPU v7x, 256 devices: a whole 4x4x8 slice. The times are simulated.
256 devices in a mesh: fs: 16 (over y, x), tp: 16 (over z, core).
Axes of the slice: x: 4, y: 4, z: 8, core: 2. Of those that a mesh axis runs over, the one named last changes fastest.
Arguments:
- normed_inputs: bfloat16 [16384, 4096], P('fs', 'tp'), may hold values from -6 to 6
- query_upstream: bfloat16 [16384, 4096], P('fs', 'tp'), may hold values from -0.0625 to 0.0625
- key_upstream: bfloat16 [16384, 1024], P('fs', 'tp'), may hold values from -0.046875 to 0.046875
- head_outputs: bfloat16 [16384, 4096], P('fs', 'tp'), may hold values from -6 to 6
- branch_upstream: bfloat16 [16384, 4096], P('fs', 'tp'), may hold values from -0.0625 to 0.0625
- query_master: float32 [4096, 4096], P('fs', 'tp'), may hold values from -0.09375 to 0.09375
- key_master: float32 [4096, 1024], P('fs', 'tp'), may hold values from -0.09375 to 0.09375
- branch_master: float32 [4096, 4096], P('fs', 'tp'), may hold values from -0.09375 to 0.09375
- query_basis: bfloat16 [4096, 128], replicated, may hold values from -0.09375 to 0.09375
- key_basis: bfloat16 [4096, 128], replicated, may hold values from -0.09375 to 0.09375
- branch_basis: bfloat16 [4096, 128], replicated, may hold values from -0.09375 to 0.09375
- query_first: float32 [128, 4096], P(None, 'tp'), may hold values from -0.75 to 0.75
- query_second: float32 [128, 4096], P(None, 'tp'), may hold values from 0.001 to 0.02
- key_first: float32 [128, 1024], P(None, 'tp'), may hold values from -0.75 to 0.75
- key_second: float32 [128, 1024], P(None, 'tp'), may hold values from 0.001 to 0.02
- branch_first: float32 [4096, 128], P('fs'), may hold values from -0.75 to 0.75
- branch_second: float32 [4096, 128], P('fs'), may hold values from 0.001 to 0.02
Outputs:
- query_step: float32 [4096, 4096], P('fs', 'tp')
- key_step: float32 [4096, 1024], P('fs', 'tp')
- branch_step: float32 [4096, 4096], P('fs', 'tp')
- query_updated: float32 [4096, 4096], P('fs', 'tp')
- key_updated: float32 [4096, 1024], P('fs', 'tp')
- branch_updated: float32 [4096, 4096], P('fs', 'tp')
- query_copy: bfloat16 [4096, 4096], P(None, 'tp')
- key_copy: bfloat16 [4096, 1024], P(None, 'tp')
- branch_copy: bfloat16 [4096, 4096], P(None, 'tp')
- query_first_new: float32 [128, 4096], P(None, 'tp')
- query_second_new: float32 [128, 4096], P(None, 'tp')
- key_first_new: float32 [128, 1024], P(None, 'tp')
- key_second_new: float32 [128, 1024], P(None, 'tp')
- branch_first_new: float32 [4096, 128], P('fs')
- branch_second_new: float32 [4096, 128], P('fs')
All inputs are finite; a program needn't handle non-finite values.
Results may differ from a plain program's by a relative error of at most 0.001.
Values may be sent and summed in bfloat16 or wider, within the bound.
A program may use at most 128 MiB of HBM per device.

v0:
```python
import functools
import jax
import jax.numpy as jnp
from jax import lax
from jax.sharding import Mesh
from jax.sharding import PartitionSpec as P

FS = ("fs_0", "fs_1")
TP = ("tp_0", "tp_1")
FS_TP = ("fs_0", "fs_1", "tp_0", "tp_1")
LEARN = 0.02
BETA_ONE = 0.9
BETA_TWO = 0.95
ADAM_EPS = 1e-08
CLIP_RMS = 0.5


def together(arrays, axis):
    vector, at, outs = (jnp.concatenate([a.reshape(-1) for a in arrays]), 0, [])
    subtotal = lax.psum(vector, axis)
    for a in arrays:
        outs.append(subtotal[at : at + a.size].reshape(a.shape))
        at += a.size
    return tuple(outs)


def in_blocks(array, dim, length):
    shape = array.shape
    pieces = array.reshape(*shape[:dim], length, shape[dim] // length, *shape[dim + 1 :])
    return jnp.moveaxis(pieces, dim, 0)


def sum_at_owner(array, axis, dim):
    pieces = in_blocks(array, dim, lax.axis_size(axis))
    arrived = lax.all_to_all(pieces, axis, split_axis=0, concat_axis=0, tiled=True)
    return arrived.sum(axis=0)


def copy_for_each(array, axis):
    length = lax.axis_size(axis)
    return lax.all_to_all(
        jnp.broadcast_to(array[None], (length, *array.shape)), axis, 0, 0, tiled=True
    )


def of_everyone(array, axis):
    return copy_for_each(array, axis).sum(axis=0)


def packed_total(arrays, axis):
    ends = [0]
    for a in arrays:
        ends.append(ends[-1] + a.size)
    subtotal = of_everyone(jnp.concatenate([a.ravel() for a in arrays]), axis)
    return tuple((subtotal[b:e].reshape(a.shape) for a, b, e in zip(arrays, ends, ends[1:])))


def gathered_total(array, axis):
    pieces = lax.all_gather(array, axis)
    return pieces.sum(axis=0)


def over_axes(array, axes):
    return functools.reduce(lax.psum, axes, array)


def in_one_piece(arrays, axis, dim, along):
    ends, at = ([], 0)
    for a in arrays[:-1]:
        at += a.shape[along]
        ends.append(at)
    both = jnp.concatenate(arrays, axis=along)
    return tuple(jnp.split(lax.all_gather(both, axis, axis=dim, tiled=True), ends, axis=along))


def moments(first, second, low, clip):
    scaled = clip * low
    first_new = BETA_ONE * first + (1.0 - BETA_ONE) * scaled
    second_new = BETA_TWO * second + (1.0 - BETA_TWO) * scaled * scaled
    return (first_new, second_new, first_new / (jnp.sqrt(second_new) + ADAM_EPS))


def over_tokens(left, right, precision=None):
    return lax.dot_general(
        left,
        right,
        (((0,), (0,)), ((), ())),
        precision=precision,
        preferred_element_type=jnp.float32,
    )


def per_device(
    normed_inputs,
    query_upstream,
    key_upstream,
    head_outputs,
    branch_upstream,
    query_master,
    key_master,
    branch_master,
    query_basis,
    key_basis,
    branch_basis,
    query_first,
    query_second,
    key_first,
    key_second,
    branch_first,
    branch_second,
):
    exact = lax.Precision.HIGHEST
    row_index = lax.axis_index(FS)
    col_index = lax.axis_index(TP)
    n_rows = lax.axis_size(FS)
    n_cols = lax.axis_size(TP)
    features = normed_inputs.shape[1]
    query_local = query_upstream.shape[1]
    key_local = key_upstream.shape[1]
    rows_in = query_master.shape[0]
    rank = query_basis.shape[1]
    whole_values = lax.all_gather(head_outputs, TP, axis=1, tiled=True)
    block_query = lax.dynamic_slice_in_dim(query_basis, col_index * features, features, 0)
    block_key = lax.dynamic_slice_in_dim(key_basis, col_index * features, features, 0)
    proj_query, proj_key = together(
        (
            jnp.dot(normed_inputs, block_query, preferred_element_type=jnp.float32),
            jnp.dot(normed_inputs, block_key, preferred_element_type=jnp.float32),
        ),
        TP,
    )
    part_query = over_tokens(proj_query, query_upstream.astype(jnp.float32), exact)
    part_key = over_tokens(proj_key, key_upstream.astype(jnp.float32), exact)
    grad_branch = sum_at_owner(over_tokens(whole_values, branch_upstream), FS, 0)
    own_branch = lax.dynamic_slice_in_dim(branch_basis, col_index * features, features, 0).astype(
        jnp.float32
    )
    part_branch = jnp.dot(grad_branch, own_branch, precision=exact)
    query_low, key_low = packed_total((part_query, part_key), FS)
    branch_low = gathered_total(part_branch, TP)
    local_squares = (jnp.sum(query_low * query_low) + jnp.sum(key_low * key_low)) / n_rows
    local_squares = local_squares + jnp.sum(branch_low * branch_low) / n_cols
    total = over_axes(local_squares, FS_TP)
    entries = rank * n_cols * (2 * query_local + key_local)
    rms_value = jnp.sqrt(total / float(entries))
    clip = 1.0 / jnp.maximum(1.0, rms_value / CLIP_RMS)
    q_first, q_second, q_dir = moments(query_first, query_second, query_low, clip)
    k_first, k_second, k_dir = moments(key_first, key_second, key_low, clip)
    b_first, b_second, b_dir = moments(branch_first, branch_second, branch_low, clip)
    step_rows_query = lax.dynamic_slice_in_dim(query_basis, row_index * rows_in, rows_in, 0).astype(
        jnp.float32
    )
    step_rows_key = lax.dynamic_slice_in_dim(key_basis, row_index * rows_in, rows_in, 0).astype(
        jnp.float32
    )
    query_step = jnp.dot(step_rows_query, q_dir, precision=exact)
    key_step = jnp.dot(step_rows_key, k_dir, precision=exact)
    branch_step = jnp.dot(b_dir, own_branch.T, precision=exact)
    query_updated = query_master - LEARN * query_step
    key_updated = key_master - LEARN * key_step
    branch_updated = branch_master - LEARN * branch_step
    query_copy, key_copy, branch_copy = in_one_piece(
        (
            query_updated.astype(jnp.bfloat16),
            key_updated.astype(jnp.bfloat16),
            branch_updated.astype(jnp.bfloat16),
        ),
        FS,
        0,
        1,
    )
    return (
        query_step,
        key_step,
        branch_step,
        query_updated,
        key_updated,
        branch_updated,
        query_copy,
        key_copy,
        branch_copy,
        q_first,
        q_second,
        k_first,
        k_second,
        b_first,
        b_second,
    )


def solution(mesh):
    finer = Mesh(mesh.devices.reshape(4, 4, 8, 2), ("fs_0", "fs_1", "tp_0", "tp_1"))
    return jax.shard_map(
        per_device,
        mesh=finer,
        in_specs=(
            P(FS, TP),
            P(FS, TP),
            P(FS, TP),
            P(FS, TP),
            P(FS, TP),
            P(FS, TP),
            P(FS, TP),
            P(FS, TP),
            P(),
            P(),
            P(),
            P(None, TP),
            P(None, TP),
            P(None, TP),
            P(None, TP),
            P(FS, None),
            P(FS, None),
        ),
        out_specs=(
            P(FS, TP),
            P(FS, TP),
            P(FS, TP),
            P(FS, TP),
            P(FS, TP),
            P(FS, TP),
            P(None, TP),
            P(None, TP),
            P(None, TP),
            P(None, TP),
            P(None, TP),
            P(None, TP),
            P(None, TP),
            P(FS, None),
            P(FS, None),
        ),
        check_vma=False,
    )
```

profile of v0, /device:TPU:2, one launch (start us, length us, event | category | flops | bytes accessed | tf_op | source)
XLA Modules:
  0.0 396.6 jit_solution(3107865244808029063)
XLA Ops:
  7.2 0.7 all-gather.5.cloned.1.call-update
  7.9 1.4 convolution_bitcast_fusion
  9.3 67.5 %all-gather.5.cloned.1.call-done = bf16[1024,4096]{1,0:T(8,128)(2,1)} async-done(((bf16[1024,256]{1,0:T(8,128)(2,1)}), bf16[1024,4096]{1,0:T(8,128)(2,1)}) %all-gather.5.cloned.1.call-update) | async-done | bytes 8388624 | tf_op jit(solution)/shard_map/all_gather | solution.py:122
  76.8 7.8 %fusion.39 = f32[4096,256]{1,0:T(8,128)} fusion(bf16[1024,4096]{1,0:T(8,128)(2,1)} %all-gather.5.cloned.1.call-done, bf16[1024,256]{1,0:T(8,128)(2,1)} %param.21), kind=kOutput, calls=%fused_computation.61 | convolution fusion | flops 2147483648 | bytes 13107200 | tf_op jit(solution)/shard_map/dot_general | solution.py:84
  84.6 7.4 %all-to-all-start.1 = ((f32[16,256,256]{2,1,0:T(8,128)}), f32[16,256,256]{2,1,0:T(8,128)}, u32[]{:S(2)}, u32[]{:S(2)}) async-start(f32[16,256,256]{2,1,0:T(8,128)} %bitcast.24), calls=%async_computation.1 | async-start | bytes 8388608 | tf_op jit(solution)/shard_map/all_to_all | solution.py:35
  92.1 0.3 convolution_bitcast_fusion.1
  92.4 0.2 copy.71
  92.6 0.2 copy.70
  92.8 1.0 pad_maximum_fusion
  94.0 58.0 %all-to-all-done.1 = f32[16,256,256]{2,1,0:T(8,128)} async-done(((f32[16,256,256]{2,1,0:T(8,128)}), f32[16,256,256]{2,1,0:T(8,128)}, u32[]{:S(2)}, u32[]{:S(2)}) %all-to-all-start.1) | async-done | bytes 4194336 | tf_op jit(solution)/shard_map/all_to_all | solution.py:35
  151.9 2.5 reduce_sum.57
  154.5 1.8 fusion.23
  156.3 52.1 %all-reduce.2.cloned.1.call-done = f32[262144]{0:T(1024)} async-done(((f32[262144]{0:T(1024)}), f32[262144]{0:T(1024)}) %all-reduce.2.cloned.1.call-update) | async-done | bytes 1048592 | tf_op jit(solution)/shard_map/psum | solution.py:20
  208.4 1.6 fusion
  210.0 0.1 reshape.96
  210.1 1.6 convolution_bitcast_fusion.2
  211.8 3.5 broadcast_in_dim.2
  215.4 7.4 %all-to-all-start = ((f32[16,1,40960]{2,1,0:T(1,128)}), f32[16,1,40960]{2,1,0:T(1,128)}, u32[]{:S(2)}, u32[]{:S(2)}) async-start(f32[16,1,40960]{2,1,0:T(1,128)} %broadcast_in_dim.2), calls=%async_computation | async-start | bytes 5242880 | tf_op jit(solution)/shard_map/all_to_all | solution.py:41
  222.9 0.1 copy.74
  223.0 34.4 %all-to-all-done = f32[16,1,40960]{2,1,0:T(1,128)} async-done(((f32[16,1,40960]{2,1,0:T(1,128)}), f32[16,1,40960]{2,1,0:T(1,128)}, u32[]{:S(2)}, u32[]{:S(2)}) %all-to-all-start) | async-done | bytes 2621472 | tf_op jit(solution)/shard_map/all_to_all | solution.py:41
  257.4 3.4 reduce_sum.54
  260.8 0.6 multiply_reduce_fusion.2
  261.4 0.6 multiply_reduce_fusion.1
  263.4 1.7 reduce_sum.58
  265.1 0.6 multiply_reduce_fusion
  266.4 0.1 copy.75
  266.5 9.4 %psum.36 = f32[]{:T(128)} all-reduce(f32[]{:T(128)S(6)} %add.73), channel_id=1, replica_groups=mesh['fs_0'=4,'fs_1'=4,'tp_0'=8,'tp_1'=2] {'fs_0'}, use_global_device_ids=true, to_apply=%region_7.0 | all-reduce | flops 1 | bytes 8 | tf_op jit(solution)/shard_map/psum | solution.py:64
  275.9 0.1 copy.76
  276.0 13.9 %psum.37 = f32[]{:T(128)} all-reduce(f32[]{:T(128)} %psum.36), channel_id=1, replica_groups=mesh['fs_0'=4,'fs_1'=4,'tp_0'=8,'tp_1'=2] {'fs_1'}, use_global_device_ids=true, to_apply=%region_8.0 | all-reduce | flops 1 | bytes 8 | tf_op jit(solution)/shard_map/psum | solution.py:64
  289.9 0.1 copy.77
  290.1 18.4 %psum.38 = f32[]{:T(128)} all-reduce(f32[]{:T(128)} %psum.37), channel_id=1, replica_groups=mesh['fs_0'=4,'fs_1'=4,'tp_0'=8,'tp_1'=2] {'tp_0'}, use_global_device_ids=true, to_apply=%region_9.0 | all-reduce | flops 1 | bytes 8 | tf_op jit(solution)/shard_map/psum | solution.py:64
  308.5 3.3 psum.39
  312.5 0.1 mul.166
  312.8 1.8 fusion.36
  314.7 0.3 fusion.35
  315.0 1.2 fusion.37
  316.2 0.7 pad_maximum_fusion.1
  316.9 0.7 copy.85
  317.6 0.7 copy.84
  318.3 0.8 copy.80
  319.2 0.8 copy.78
  320.0 0.8 copy.81
  320.9 0.8 copy.79
  321.7 56.1 %all-gather.7.cloned.1.call-done = bf16[4096,576]{0,1:T(8,128)(2,1)} async-done(((bf16[256,576]{0,1:T(8,128)(2,1)}), bf16[4096,576]{0,1:T(8,128)(2,1)}) %all-gather.7.cloned.1.call-update) | async-done | bytes 4718608 | tf_op jit(solution)/shard_map/all_gather | solution.py:73
  377.8 3.9 fusion.38
  381.7 4.1 %copy.83 = bf16[4096,256]{1,0:T(8,128)(2,1)} copy(bf16[4096,256]{0,1:T(8,128)(2,1)} %get-tuple-element.81) | data formatting | bytes 4194304
  385.8 2.4 copy.82
  388.2 1.9 split.13
  (50 shorter events, 0.6 us)
Async XLA Ops:
  7.2 84.9 %copy-start = (bf16[4096,128]{1,0:T(8,128)(2,1)S(1)}, bf16[4096,128]{1,0:T(8,128)(2,1)}, u32[]{:S(2)}) copy-start(bf16[4096,128]{1,0:T(8,128)(2,1)} %param.25) | copy-start | bytes 3145732
  7.2 69.6 %all-gather.5.cloned.1.call-start = ((), (), s32[]{:S(2)}) async-start(), calls=%async_computation.3 | async-start | bytes 8912896 | tf_op jit(solution)/shard_map/all_gather | solution.py:122
  84.6 7.5 %copy-start.1 = (bf16[1024,256]{1,0:T(8,128)(2,1)S(1)}, bf16[1024,256]{1,0:T(8,128)(2,1)}, u32[]{:S(2)}) copy-start(bf16[1024,256]{1,0:T(8,128)(2,1)} %param.17) | copy-start | bytes 1572868
  84.6 67.3 %all-to-all-start.1 = ((f32[16,256,256]{2,1,0:T(8,128)}), f32[16,256,256]{2,1,0:T(8,128)}, u32[]{:S(2)}, u32[]{:S(2)}) async-start(f32[16,256,256]{2,1,0:T(8,128)} %bitcast.24), calls=%async_computation.1 | async-start | bytes 8388608 | tf_op jit(solution)/shard_map/all_to_all | solution.py:35
  92.0 116.3 %all-reduce.2.cloned.1.call-start = ((), (), s32[]{:S(2)}) async-start(), calls=%async_computation.2 | async-start | bytes 2097152 | tf_op jit(solution)/shard_map/psum | solution.py:20
  92.8 115.6 %copy-start.11 = (bf16[1024,64]{0,1:T(8,128)(2,1)S(1)}, bf16[1024,64]{0,1:T(8,128)(2,1)}, u32[]{:S(2)}) copy-start(bf16[1024,64]{0,1:T(8,128)(2,1)} %param.19) | copy-start | bytes 393220
  92.8 117.3 %copy-start.4 = (bf16[1024,256]{1,0:T(8,128)(2,1)S(1)}, bf16[1024,256]{1,0:T(8,128)(2,1)}, u32[]{:S(2)}) copy-start(bf16[1024,256]{1,0:T(8,128)(2,1)} %param.18) | copy-start | bytes 1572868
  93.9 169.5 %all-gather.9.cloned.1.call-start = ((), (), s32[]{:S(2)}) async-start(), calls=%async_computation.5 | async-start | bytes 2228224 | tf_op jit(solution)/shard_map/all_gather | solution.py:59
  211.8 11.1 %copy-start.15 = (f32[128,64]{0,1:T(8,128)S(1)}, f32[128,64]{0,1:T(8,128)}, u32[]{:S(2)}) copy-start(f32[128,64]{0,1:T(8,128)} %param.30) | copy-start | bytes 98308
  215.4 51.0 %copy-start.16 = (f32[128,64]{0,1:T(8,128)S(1)}, f32[128,64]{0,1:T(8,128)}, u32[]{:S(2)}) copy-start(f32[128,64]{0,1:T(8,128)} %param.31) | copy-start | bytes 98308
  215.4 60.5 %copy-start.7 = (f32[256,256]{1,0:T(8,128)S(1)}, f32[256,256]{1,0:T(8,128)}, u32[]{:S(2)}) copy-start(f32[256,256]{1,0:T(8,128)} %param.22) | copy-start | bytes 786436
  215.4 42.0 %all-to-all-start = ((f32[16,1,40960]{2,1,0:T(1,128)}), f32[16,1,40960]{2,1,0:T(1,128)}, u32[]{:S(2)}, u32[]{:S(2)}) async-start(f32[16,1,40960]{2,1,0:T(1,128)} %broadcast_in_dim.2), calls=%async_computation | async-start | bytes 5242880 | tf_op jit(solution)/shard_map/all_to_all | solution.py:41
  222.8 67.2 %copy-start.8 = (f32[256,256]{1,0:T(8,128)S(1)}, f32[256,256]{1,0:T(8,128)}, u32[]{:S(2)}) copy-start(f32[256,256]{1,0:T(8,128)} %param.24) | copy-start | bytes 786436
  222.8 89.8 %copy-start.12 = (f32[256,128]{1,0:T(8,128)S(1)}, f32[256,128]{1,0:T(8,128)}, u32[]{:S(2)}) copy-start(f32[256,128]{1,0:T(8,128)} %param.33) | copy-start | bytes 393220
  222.8 89.8 %copy-start.13 = (f32[256,128]{1,0:T(8,128)S(1)}, f32[256,128]{1,0:T(8,128)}, u32[]{:S(2)}) copy-start(f32[256,128]{1,0:T(8,128)} %param.32) | copy-start | bytes 393220
  222.8 89.9 %copy-start.9 = (f32[128,256]{1,0:T(8,128)S(1)}, f32[128,256]{1,0:T(8,128)}, u32[]{:S(2)}) copy-start(f32[128,256]{1,0:T(8,128)} %param.29) | copy-start | bytes 393220
  222.8 89.9 %copy-start.10 = (f32[128,256]{1,0:T(8,128)S(1)}, f32[128,256]{1,0:T(8,128)}, u32[]{:S(2)}) copy-start(f32[128,256]{1,0:T(8,128)} %param.28) | copy-start | bytes 393220
  222.8 154.9 %all-gather.7.cloned.1.call-start = ((), (), s32[]{:S(2)}) async-start(), calls=%async_computation.4 | async-start | bytes 5013504 | tf_op jit(solution)/shard_map/all_gather | solution.py:73
  223.0 89.8 %copy-start.14 = (f32[256,64]{0,1:T(8,128)S(1)}, f32[256,64]{0,1:T(8,128)}, u32[]{:S(2)}) copy-start(f32[256,64]{0,1:T(8,128)} %param.23) | copy-start | bytes 196612
  312.7 9.0 %copy-start.6 = (f32[256,128]{1,0:T(8,128)}, f32[256,128]{1,0:T(8,128)S(1)}, u32[]{:S(2)}) copy-start(f32[256,128]{1,0:T(8,128)S(1)} %get-tuple-element.84) | copy-start | bytes 393220
  312.7 69.0 %copy-start.5 = (f32[256,128]{1,0:T(8,128)}, f32[256,128]{1,0:T(8,128)S(1)}, u32[]{:S(2)}) copy-start(f32[256,128]{1,0:T(8,128)S(1)} %get-tuple-element.83) | copy-start | bytes 393220
  312.8 68.9 %copy-start.2 = (f32[128,256]{1,0:T(8,128)}, f32[128,256]{1,0:T(8,128)S(1)}, u32[]{:S(2)}) copy-start(f32[128,256]{1,0:T(8,128)S(1)} %get-tuple-element.85) | copy-start | bytes 393220
  312.8 68.9 %copy-start.3 = (f32[128,256]{1,0:T(8,128)}, f32[128,256]{1,0:T(8,128)S(1)}, u32[]{:S(2)}) copy-start(f32[128,256]{1,0:T(8,128)S(1)} %get-tuple-element.86) | copy-start | bytes 393220
Sparse Core Ops, SparseCore 0:
  9.8 66.9 all-gather.4
  95.8 112.5 all-reduce.1
  210.8 39.7 all-gather.8
  317.1 60.6 all-gather.6
where the time goes:
time: 397 us
  waiting for transfers between devices  269 us (68%)
  blocking collectives  45 us (11%)
  local copies, waits for them, and re-layouts  21.8 us (5%)
  matrix products  17.9 us (5%)
  between operations  16.8 us (4%)
  starting transfers between devices  15 us (4%)
  other arithmetic  11.4 us (3%)
    all_gather x1, waiting for transfers between devices, per_device(): whole_values = lax.all_gather(head_outputs, TP, axis=1, tiled=True)  67.5 us
    all_to_all x1, waiting for transfers between devices, sum_at_owner(): lax.all_to_all(pieces, axis, split_axis=0, concat_axis=0, tiled=True)  58 us
    all_gather x1, waiting for transfers between devices, in_one_piece(): lax.all_gather(both, axis, axis=dim, tiled=True)  56.1 us
    psum x1, waiting for transfers between devices, together(): subtotal = lax.psum(vector, axis)  52.1 us
    psum x4, blocking collectives, over_axes(): return functools.reduce(lax.psum, axes, array)  45 us
    all_to_all x1, waiting for transfers between devices, copy_for_each(): lax.all_to_all(jnp.broadcast_to(array[None], (length, *array.shape)), axi...  34.4 us
    unnamed x47, local copies, waits for them, and re-layouts  11.9 us
    dot_general x3, matrix products, over_tokens(): lax.dot_general(left, right, (((0,), (0,)), ((), ())), precision=precisio...  11.1 us
  transfers between devices with their start and end apart: 6, of which 5 were waited for; matrix products, arithmetic and copies ran while one was open for 6% of the time, Pallas kernels for 0%

commit v1 on v0

--- a/solution.py
+++ b/solution.py
@@ -17,7 +17,7 @@
 
 def together(arrays, axis):
     vector, at, outs = (jnp.concatenate([a.reshape(-1) for a in arrays]), 0, [])
-    subtotal = lax.psum(vector, axis)
+    subtotal = jnp.sum(lax.all_gather(vector, axis), axis=0)
     for a in arrays:
         outs.append(subtotal[at : at + a.size].reshape(a.shape))
         at += a.size

time: 397 us -> 386 us (0.972)
  waiting for transfers between devices: 269 us -> 183 us
  blocking collectives: 45 us -> 99.1 us
  local copies, waits for them, and re-layouts: 21.8 us -> 38.3 us
  other arithmetic: 11.4 us -> 24.5 us
  starting transfers between devices: 15 us -> 7.61 us
    all_to_all x1 -> x0, waiting for transfers between devices: 58 us -> none  [sum_at_owner(): lax.all_to_all(pieces, axis, split_axis=0, concat_axis=0, tiled=True)]
    all_to_all x0 -> x1, blocking collectives: none -> 57.1 us  [sum_at_owner(): lax.all_to_all(pieces, axis, split_axis=0, concat_axis=0, tiled=True)]
    psum x1 -> x0, waiting for transfers between devices: 52.1 us -> none  [together(): subtotal = lax.psum(vector, axis)]
    all_gather x0 -> x1, waiting for transfers between devices: none -> 29.2 us  [together(): subtotal = jnp.sum(lax.all_gather(vector, axis), axis=0)]
    all_gather x0 -> x1, local copies, waits for them, and re-layouts: none -> 16.2 us  [together(): subtotal = jnp.sum(lax.all_gather(vector, axis), axis=0)]
    reduce_sum x0 -> x1, other arithmetic: none -> 13.1 us  [together(): subtotal = jnp.sum(lax.all_gather(vector, axis), axis=0)]
    all_to_all x1 -> x0, starting transfers between devices: 7.41 us -> none  [sum_at_owner(): lax.all_to_all(pieces, axis, split_axis=0, concat_axis=0, tiled=True)]
    dot_general x3, matrix products: 11.1 us -> 7.13 us  [over_tokens(): lax.dot_general(left, right, (((0,), (0,)), ((), ())), precision=precisio...]
  transfers between devices with their start and end apart: 6 -> 5, of which waited for: 5 -> 4; matrix products, arithmetic and copies ran while one was open for 6% -> 14% of each run, Pallas kernels for 0% -> 0%
where the time goes in v1:
time: 386 us; the launch traced here: 385 us
  waiting for transfers between devices  183 us (47%)
  blocking collectives  99.1 us (26%)
  local copies, waits for them, and re-layouts  38.3 us (10%)
  other arithmetic  24.5 us (6%)
  between operations  16.8 us (4%)
  matrix products  15.1 us (4%)
  starting transfers between devices  7.61 us (2%)
    all_gather x1, waiting for transfers between devices, per_device(): whole_values = lax.all_gather(head_outputs, TP, axis=1, tiled=True)  64.1 us
    all_to_all x1, blocking collectives, sum_at_owner(): lax.all_to_all(pieces, axis, split_axis=0, concat_axis=0, tiled=True)  57.1 us
    all_gather x1, waiting for transfers between devices, in_one_piece(): lax.all_gather(both, axis, axis=dim, tiled=True)  55.4 us
    psum x4, blocking collectives, over_axes(): return functools.reduce(lax.psum, axes, array)  42.1 us
    all_to_all x1, waiting for transfers between devices, copy_for_each(): lax.all_to_all(jnp.broadcast_to(array[None], (length, *array.shape)), axi...  33.8 us
    all_gather x1, waiting for transfers between devices, together(): subtotal = jnp.sum(lax.all_gather(vector, axis), axis=0)  29.2 us
    all_gather x1, local copies, waits for them, and re-layouts, together(): subtotal = jnp.sum(lax.all_gather(vector, axis), axis=0)  16.2 us
    reduce_sum x1, other arithmetic, together(): subtotal = jnp.sum(lax.all_gather(vector, axis), axis=0)  13.1 us
  transfers between devices with their start and end apart: 5, of which 4 were waited for; matrix products, arithmetic and copies ran while one was open for 14% of the time, Pallas kernels for 0%

profile of v1, /device:TPU:2, one launch (start us, length us, event | category | flops | bytes accessed | tf_op | source)
XLA Modules:
  0.0 384.8 jit_solution(8350071058203103279)
XLA Ops:
  7.2 0.7 all-gather.7.cloned.1.call-update
  8.0 0.4 copy-done
  8.4 1.3 convolution_bitcast_fusion.1
  9.8 0.2 copy.85
  10.0 1.4 convolution_bitcast_fusion
  11.4 0.2 copy.86
  11.6 1.0 pad_maximum_fusion
  12.7 64.1 %all-gather.7.cloned.1.call-done = bf16[1024,4096]{1,0:T(8,128)(2,1)} async-done(((bf16[1024,256]{1,0:T(8,128)(2,1)}), bf16[1024,4096]{1,0:T(8,128)(2,1)}) %all-gather.7.cloned.1.call-update) | async-done | bytes 8388624 | tf_op jit(solution)/shard_map/all_gather | solution.py:122
  76.8 6.0 %fusion.39 = f32[4096,256]{1,0:T(8,128)S(1)} fusion(bf16[1024,4096]{1,0:T(8,128)(2,1)} %all-gather.7.cloned.1.call-done, bf16[1024,256]{1,0:T(8,128)(2,1)S(1)} %copy-done.15), kind=kOutput, calls=%fused_computation.61 | convolution fusion | flops 2147483648 | bytes 13107200 | tf_op jit(solution)/shard_map/dot_general | solution.py:84
  82.8 57.1 %all_to_all.11 = f32[16,256,256]{2,1,0:T(8,128)} all-to-all(f32[16,256,256]{2,1,0:T(8,128)S(1)} %bitcast.24), channel_id=1, replica_groups=mesh['fs_0'=4,'fs_1'=4,'tp_0'=8,'tp_1'=2] {'fs_0','fs_1'}, dimensions={0} | all-to-all | bytes 8388608 | tf_op jit(solution)/shard_map/all_to_all | solution.py:35
  139.8 2.5 reduce_sum.67
  142.3 1.8 fusion.23
  144.1 29.2 %all-gather.11.cloned.1.call-done = f32[4194304]{0:T(1024)} async-done(((f32[262144]{0:T(1024)}), f32[4194304]{0:T(1024)}) %all-gather.11.cloned.1.call-update) | async-done | bytes 16777232 | tf_op jit(solution)/shard_map/all_gather | solution.py:20
  173.3 16.2 %reshape.98 = f32[16,262144]{1,0:T(8,128)} reshape(f32[4194304]{0:T(1024)} %all-gather.11.cloned.1.call-done) | data formatting | bytes 33554432 | tf_op jit(solution)/shard_map/all_gather | solution.py:20
  189.4 13.1 %reduce_sum.63 = f32[262144]{0:T(1024)S(1)} reduce(f32[16,262144]{1,0:T(8,128)} %reshape.98, f32[]{:T(128)} %constant.11.clone.1), dimensions={0}, to_apply=%region_0.0 | reduce | flops 3932160 | bytes 17825796 | tf_op jit(solution)/shard_map/reduce_sum | solution.py:20
  202.6 0.6 convolution_bitcast_fusion.2
  203.2 0.6 fusion
  203.9 3.5 broadcast_in_dim.2
  207.5 7.3 %all-to-all-start = ((f32[16,1,40960]{2,1,0:T(1,128)}), f32[16,1,40960]{2,1,0:T(1,128)}, u32[]{:S(2)}, u32[]{:S(2)}) async-start(f32[16,1,40960]{2,1,0:T(1,128)} %broadcast_in_dim.2), calls=%async_computation | async-start | bytes 5242880 | tf_op jit(solution)/shard_map/all_to_all | solution.py:41
  214.8 0.2 all-gather.9.cloned.1.call-start
  215.0 0.1 copy.92
  215.2 1.7 reduce_sum.68
  217.0 0.6 multiply_reduce_fusion
  217.6 33.8 %all-to-all-done = f32[16,1,40960]{2,1,0:T(1,128)} async-done(((f32[16,1,40960]{2,1,0:T(1,128)}), f32[16,1,40960]{2,1,0:T(1,128)}, u32[]{:S(2)}, u32[]{:S(2)}) %all-to-all-start) | async-done | bytes 2621472 | tf_op jit(solution)/shard_map/all_to_all | solution.py:41
  251.4 3.4 reduce_sum.64
  254.8 0.6 multiply_reduce_fusion.1
  255.5 0.6 multiply_reduce_fusion.2
  258.0 0.1 copy.89
  258.1 9.7 %psum.28 = f32[]{:T(128)} all-reduce(f32[]{:T(128)S(6)} %add.71), channel_id=1, replica_groups=mesh['fs_0'=4,'fs_1'=4,'tp_0'=8,'tp_1'=2] {'fs_0'}, use_global_device_ids=true, to_apply=%region_7.0 | all-reduce | flops 1 | bytes 8 | tf_op jit(solution)/shard_map/psum | solution.py:64
  267.9 13.1 %psum.29 = f32[]{:T(128)} all-reduce(f32[]{:T(128)} %psum.28), channel_id=1, replica_groups=mesh['fs_0'=4,'fs_1'=4,'tp_0'=8,'tp_1'=2] {'fs_1'}, use_global_device_ids=true, to_apply=%region_8.0 | all-reduce | flops 1 | bytes 8 | tf_op jit(solution)/shard_map/psum | solution.py:64
  281.0 0.1 copy.91
  281.1 16.2 %psum.30 = f32[]{:T(128)} all-reduce(f32[]{:T(128)} %psum.29), channel_id=1, replica_groups=mesh['fs_0'=4,'fs_1'=4,'tp_0'=8,'tp_1'=2] {'tp_0'}, use_global_device_ids=true, to_apply=%region_9.0 | all-reduce | flops 1 | bytes 8 | tf_op jit(solution)/shard_map/psum | solution.py:64
  297.3 3.1 psum.31
  301.4 1.2 fusion.37
  302.8 1.9 fusion.36
  304.6 0.3 fusion.35
  305.0 0.7 pad_maximum_fusion.1
  305.7 0.7 copy.100
  306.4 0.7 copy.99
  307.1 0.8 copy.94
  308.0 0.8 copy.96
  308.8 0.8 copy.93
  309.7 0.8 copy.95
  310.5 55.4 %all-gather.9.cloned.1.call-done = bf16[4096,576]{0,1:T(8,128)(2,1)} async-done(((bf16[256,576]{0,1:T(8,128)(2,1)}), bf16[4096,576]{0,1:T(8,128)(2,1)}) %all-gather.9.cloned.1.call-update) | async-done | bytes 4718608 | tf_op jit(solution)/shard_map/all_gather | solution.py:73
  365.9 3.9 %fusion.38 = (bf16[4096,256]{0,1:T(8,128)(2,1)S(1)}, bf16[4096,256]{0,1:T(8,128)(2,1)}) fusion(bf16[4096,576]{0,1:T(8,128)(2,1)} %all-gather.9.cloned.1.call-done), kind=kLoop, calls=%fused_computation.60 | loop fusion | bytes 8388608 | tf_op jit(solution)/shard_map/split | solution.py:73
  369.9 4.1 %copy.97 = bf16[4096,256]{1,0:T(8,128)(2,1)} copy(bf16[4096,256]{0,1:T(8,128)(2,1)} %get-tuple-element.97) | data formatting | bytes 4194304
  373.9 2.4 copy.98
  376.4 1.9 split.13
  (49 shorter events, 0.8 us)
Async XLA Ops:
  7.2 1.2 copy-start
  7.2 69.6 %copy-start.15 = (bf16[1024,256]{1,0:T(8,128)(2,1)S(1)}, bf16[1024,256]{1,0:T(8,128)(2,1)}, u32[]{:S(2)}) copy-start(bf16[1024,256]{1,0:T(8,128)(2,1)} %param.21) | copy-start | bytes 1572868
  7.2 69.6 %all-gather.7.cloned.1.call-start = ((), (), s32[]{:S(2)}) async-start(), calls=%async_computation.2 | async-start | bytes 8912896 | tf_op jit(solution)/shard_map/all_gather | solution.py:122
  7.9 165.4 %all-gather.11.cloned.1.call-start = ((), (), s32[]{:S(2)}) async-start(), calls=%async_computation.4 | async-start | bytes 17825792 | tf_op jit(solution)/shard_map/all_gather | solution.py:20
  12.6 202.6 %all-gather.13.cloned.1.call-start = ((), (), s32[]{:S(2)}) async-start(), calls=%async_computation.5 | async-start | bytes 2228224 | tf_op jit(solution)/shard_map/all_gather | solution.py:59
  189.4 13.1 %copy-start.3 = (bf16[1024,256]{1,0:T(8,128)(2,1)S(1)}, bf16[1024,256]{1,0:T(8,128)(2,1)}, u32[]{:S(2)}) copy-start(bf16[1024,256]{1,0:T(8,128)(2,1)} %param.18) | copy-start | bytes 1572868
  189.4 13.8 %copy-start.10 = (bf16[1024,64]{0,1:T(8,128)(2,1)S(1)}, bf16[1024,64]{0,1:T(8,128)(2,1)}, u32[]{:S(2)}) copy-start(bf16[1024,64]{0,1:T(8,128)(2,1)} %param.19) | copy-start | bytes 393220
  203.9 11.1 %copy-start.6 = (f32[256,256]{1,0:T(8,128)S(1)}, f32[256,256]{1,0:T(8,128)}, u32[]{:S(2)}) copy-start(f32[256,256]{1,0:T(8,128)} %param.24) | copy-start | bytes 786436
  207.5 43.9 %all-to-all-start = ((f32[16,1,40960]{2,1,0:T(1,128)}), f32[16,1,40960]{2,1,0:T(1,128)}, u32[]{:S(2)}, u32[]{:S(2)}) async-start(f32[16,1,40960]{2,1,0:T(1,128)} %broadcast_in_dim.2), calls=%async_computation | async-start | bytes 5242880 | tf_op jit(solution)/shard_map/all_to_all | solution.py:41
  214.7 43.3 %copy-start.13 = (f32[128,64]{0,1:T(8,128)S(1)}, f32[128,64]{0,1:T(8,128)}, u32[]{:S(2)}) copy-start(f32[128,64]{0,1:T(8,128)} %param.30) | copy-start | bytes 98308
  214.7 53.1 %copy-start.14 = (f32[128,64]{0,1:T(8,128)S(1)}, f32[128,64]{0,1:T(8,128)}, u32[]{:S(2)}) copy-start(f32[128,64]{0,1:T(8,128)} %param.31) | copy-start | bytes 98308
  214.7 66.3 %copy-start.7 = (f32[256,256]{1,0:T(8,128)S(1)}, f32[256,256]{1,0:T(8,128)}, u32[]{:S(2)}) copy-start(f32[256,256]{1,0:T(8,128)} %param.22) | copy-start | bytes 786436
  214.8 86.5 %copy-start.11 = (f32[256,128]{1,0:T(8,128)S(1)}, f32[256,128]{1,0:T(8,128)}, u32[]{:S(2)}) copy-start(f32[256,128]{1,0:T(8,128)} %param.33) | copy-start | bytes 393220
  214.8 86.5 %copy-start.12 = (f32[256,128]{1,0:T(8,128)S(1)}, f32[256,128]{1,0:T(8,128)}, u32[]{:S(2)}) copy-start(f32[256,128]{1,0:T(8,128)} %param.32) | copy-start | bytes 393220
  214.8 151.1 %all-gather.9.cloned.1.call-start = ((), (), s32[]{:S(2)}) async-start(), calls=%async_computation.3 | async-start | bytes 5013504 | tf_op jit(solution)/shard_map/all_gather | solution.py:73
  215.2 87.5 %copy-start.8 = (f32[128,256]{1,0:T(8,128)S(1)}, f32[128,256]{1,0:T(8,128)}, u32[]{:S(2)}) copy-start(f32[128,256]{1,0:T(8,128)} %param.29) | copy-start | bytes 393220
  215.2 87.5 %copy-start.9 = (f32[128,256]{1,0:T(8,128)S(1)}, f32[128,256]{1,0:T(8,128)}, u32[]{:S(2)}) copy-start(f32[128,256]{1,0:T(8,128)} %param.28) | copy-start | bytes 393220
  301.4 3.3 copy-start.5
  301.4 68.5 %copy-start.4 = (f32[256,128]{1,0:T(8,128)}, f32[256,128]{1,0:T(8,128)S(1)}, u32[]{:S(2)}) copy-start(f32[256,128]{1,0:T(8,128)S(1)} %get-tuple-element.98) | copy-start | bytes 393220
  302.7 67.1 %copy-start.1 = (f32[128,256]{1,0:T(8,128)}, f32[128,256]{1,0:T(8,128)S(1)}, u32[]{:S(2)}) copy-start(f32[128,256]{1,0:T(8,128)S(1)} %get-tuple-element.100) | copy-start | bytes 393220
  302.8 67.1 %copy-start.2 = (f32[128,256]{1,0:T(8,128)}, f32[128,256]{1,0:T(8,128)S(1)}, u32[]{:S(2)}) copy-start(f32[128,256]{1,0:T(8,128)S(1)} %get-tuple-element.101) | copy-start | bytes 393220
Sparse Core Ops, SparseCore 0:
  9.8 66.9 all-gather.6
  79.2 94.0 all-gather.10
  175.7 37.9 all-gather.12
  305.9 60.0 all-gather.8
